TPU v7x, 32 devices: a whole 2x2x4 slice. The times are simulated.
32 devices in a mesh: rep: 2 (over x), fs: 8 (over z, y), tp: 2 (over core).
Axes of the slice: x: 2, y: 2, z: 4, core: 2. Of those that a mesh axis runs over, the one named last changes fastest.
Arguments:
- x_early: bfloat16 [1792, 2048], P(('rep', 'fs')), may hold values from -6 to 6
- x_late: bfloat16 [1792, 2048], P(('rep', 'fs')), may hold values from -6 to 6
- grad_out: bfloat16 [1792, 2048], P(('rep', 'fs')), may hold values from -6 to 6
- w_gate: bfloat16 [2048, 3072], P('fs', 'tp'), may hold values from -0.125 to 0.125
- w_up: bfloat16 [2048, 3072], P('fs', 'tp'), may hold values from -0.125 to 0.125
- w_down: bfloat16 [3072, 2048], P('tp', 'fs'), may hold values from -0.109375 to 0.109375
- gate_sum: float32 [2048, 3072], P('fs', 'tp'), may hold values from -80 to 80
- up_sum: float32 [2048, 3072], P('fs', 'tp'), may hold values from -80 to 80
- down_sum: float32 [3072, 2048], P('tp', 'fs'), may hold values from -80 to 80
Outputs:
- out_late: bfloat16 [1792, 2048], P(('rep', 'fs'))
- grad_in: bfloat16 [1792, 2048], P(('rep', 'fs'))
- new_gate_sum: float32 [2048, 3072], P('fs', 'tp')
- new_up_sum: float32 [2048, 3072], P('fs', 'tp')
- new_down_sum: float32 [3072, 2048], P('tp', 'fs')
All inputs are finite; a program needn't handle non-finite values.
Results may differ from a plain program's by a relative error of at most 0.018.
Values may be sent and summed in bfloat16 or wider, within the bound.
A program may use at most 128 MiB of HBM per device.

v0:
```python
import jax
import jax.numpy as jnp
from jax import lax
from jax.sharding import PartitionSpec as P

epsilon = 1e-06


def contract_rows(left, right):
    return lax.dot_general(
        left, right, (((0,), (0,)), ((), ())), preferred_element_type=jnp.float32
    )


def contract_cols(left, right):
    return lax.dot_general(
        left, right, (((1,), (1,)), ((), ())), preferred_element_type=jnp.float32
    )


def shards(x_early, x_late, grad_out, w_gate, w_up, w_down, gate_sum, up_sum, down_sum):
    gate_full, up_full, down_full = (
        lax.all_gather(w_gate, "fs", axis=0, tiled=True),
        lax.all_gather(w_up, "fs", axis=0, tiled=True),
        lax.all_gather(w_down, "fs", axis=1, tiled=True),
    )
    batch_rows = x_early.shape[0]
    stacked = jnp.concatenate([x_early, x_late], axis=0).astype(jnp.float32)
    row_scale = lax.rsqrt(jnp.mean(stacked * stacked, axis=-1, keepdims=True) + epsilon)
    normed = (stacked * row_scale).astype(jnp.bfloat16)
    gate_pre = jnp.dot(normed, gate_full, preferred_element_type=jnp.float32)
    up_pre = jnp.dot(normed, up_full, preferred_element_type=jnp.float32)
    gate_sig = jax.nn.sigmoid(gate_pre)
    hidden = (gate_pre * gate_sig * up_pre).astype(jnp.bfloat16)
    late_part = jnp.dot(hidden[batch_rows:], down_full, preferred_element_type=jnp.float32).astype(
        jnp.bfloat16
    )
    branch = lax.psum(late_part, "tp").astype(jnp.float32)
    out_late = (stacked[batch_rows:] + 0.5 * branch).astype(jnp.bfloat16)
    early_gate = gate_pre[:batch_rows]
    early_upper = up_pre[:batch_rows]
    early_sig = gate_sig[:batch_rows]
    early_hidden = hidden[:batch_rows]
    early_normed = normed[:batch_rows]
    early_scale = row_scale[:batch_rows]
    grad_hidden = 0.5 * contract_cols(grad_out, down_full)
    grad_gate_in = (
        grad_hidden * early_upper * early_sig * (1.0 + early_gate * (1.0 - early_sig))
    ).astype(jnp.bfloat16)
    grad_up_in = (grad_hidden * early_gate * early_sig).astype(jnp.bfloat16)
    normed_part = contract_cols(grad_gate_in, gate_full) + contract_cols(grad_up_in, up_full)
    grad_normed = lax.psum(normed_part.astype(jnp.bfloat16), "tp").astype(jnp.float32)
    unit_rows = stacked[:batch_rows] * early_scale
    inner = jnp.mean(grad_normed * unit_rows, axis=-1, keepdims=True)
    grad_in = (
        grad_out.astype(jnp.float32) + early_scale * (grad_normed - unit_rows * inner)
    ).astype(jnp.bfloat16)
    normed_cols, out_cols = (
        lax.all_to_all(early_normed, "fs", split_axis=1, concat_axis=0, tiled=True),
        lax.all_to_all(grad_out, "fs", split_axis=1, concat_axis=0, tiled=True),
    )
    gate_delta = contract_rows(normed_cols, lax.all_gather(grad_gate_in, "fs", axis=0, tiled=True))
    up_delta = contract_rows(normed_cols, lax.all_gather(grad_up_in, "fs", axis=0, tiled=True))
    down_half = contract_rows(lax.all_gather(early_hidden, "fs", axis=0, tiled=True), out_cols)
    down_delta = 0.5 * down_half
    gate_delta, up_delta, down_delta = (
        lax.psum(gate_delta.astype(jnp.bfloat16), "rep").astype(jnp.float32),
        lax.psum(up_delta.astype(jnp.bfloat16), "rep").astype(jnp.float32),
        lax.psum(down_delta.astype(jnp.bfloat16), "rep").astype(jnp.float32),
    )
    return (out_late, grad_in, gate_sum + gate_delta, up_sum + up_delta, down_sum + down_delta)


def solution(mesh):
    placed = (
        P(("rep", "fs"), None),
        P(("rep", "fs"), None),
        P(("rep", "fs"), None),
        P("fs", "tp"),
        P("fs", "tp"),
        P("tp", "fs"),
        P("fs", "tp"),
        P("fs", "tp"),
        P("tp", "fs"),
    )
    return jax.shard_map(
        shards,
        mesh=mesh,
        in_specs=placed,
        out_specs=(
            P(("rep", "fs"), None),
            P(("rep", "fs"), None),
            P("fs", "tp"),
            P("fs", "tp"),
            P("tp", "fs"),
        ),
        check_vma=False,
    )
```

profile of v0, /device:TPU:0, one launch (start us, length us, event | category | flops | bytes accessed | tf_op | source)
XLA Modules:
  0.0 608.1 jit_solution(10017036902288530399)
XLA Ops:
  7.2 0.7 all-gather.9.cloned.1.call-update
  8.0 0.7 all-gather.7.cloned.1.call-update
  8.7 0.7 all-gather.11.cloned.1.call-update
  10.0 101.6 %all-gather.9.cloned.1.call-done = bf16[2048,1536]{1,0:T(8,128)(2,1)} async-done(((bf16[256,1536]{1,0:T(8,128)(2,1)}), bf16[2048,1536]{1,0:T(8,128)(2,1)}) %all-gather.9.cloned.1.call-update) | async-done | bytes 6291472 | tf_op jit(solution)/shard_map/all_gather | solution.py:24
  111.6 5.4 fusion.11
  117.1 93.6 %all-gather.7.cloned.1.call-done = bf16[2048,1536]{1,0:T(8,128)(2,1)} async-done(((bf16[256,1536]{1,0:T(8,128)(2,1)}), bf16[2048,1536]{1,0:T(8,128)(2,1)}) %all-gather.7.cloned.1.call-update) | async-done | bytes 6291472 | tf_op jit(solution)/shard_map/all_gather | solution.py:23
  210.7 6.5 %add_divide_fusion = (f32[224,1536]{1,0:T(8,128)}, bf16[224,1536]{1,0:T(8,128)(2,1)}, f32[224,1536]{1,0:T(8,128)}) fusion(f32[224,1536]{1,0:T(8,128)} %fusion.11, bf16[224,2048]{1,0:T(8,128)(2,1)S(1)} %multiply_convert_fusion, bf16[2048,1536]{1,0:T(8,128)(2,1)} %all-gather.7.cloned.1.call-done), kind=kOutput, calls=%fused_computation.14 | convolution fusion | flops 1411350528 | bytes 12025856 | tf_op jit(solution)/shard_map/dot_general | solution.py:31
  217.3 93.2 %all-gather.11.cloned.1.call-done = bf16[1536,2048]{1,0:T(8,128)(2,1)} async-done(((bf16[1536,256]{1,0:T(8,128)(2,1)}), bf16[1536,2048]{1,0:T(8,128)(2,1)}) %all-gather.11.cloned.1.call-update) | async-done | bytes 6291472 | tf_op jit(solution)/shard_map/all_gather | solution.py:25
  310.5 6.4 %multiply_convert_fusion.2 = (bf16[112,1536]{1,0:T(8,128)(2,1)}, bf16[112,1536]{1,0:T(8,128)(2,1)}) fusion(f32[224,1536]{1,0:T(8,128)} %get-tuple-element.16, f32[224,1536]{1,0:T(8,128)} %get-tuple-element.14, f32[224,1536]{1,0:T(8,128)} %fusion.11, bf16[112,2048]{1,0:T(8,128)(2,1)S(1)} %copy-done, bf16[1536,2048]{1,0:T(8,128)(2,1)} %all-gather.11.cloned.1.call-done), kind=kOutput, calls=%fused_computation.29 | convolution fusion | flops 706535424 | bytes 9502720 | tf_op jit(solution)/shard_map/dot_general | solution.py:16
  317.0 0.5 all-gather.15.cloned.1.call-update
  317.6 1.9 slice.44
  319.5 1.0 slice.43
  320.5 0.8 copy.24
  321.3 4.1 all-to-all-start
  325.5 0.8 copy.23
  326.3 5.1 fusion.12
  331.4 2.8 fusion.1
  334.2 13.9 %all-to-all-done = bf16[112,8,256]{2,0,1:T(8,128)(2,1)} async-done(((bf16[112,8,256]{2,0,1:T(8,128)(2,1)}), bf16[112,8,256]{2,0,1:T(8,128)(2,1)}, u32[]{:S(2)}, u32[]{:S(2)}) %all-to-all-start) | async-done | bytes 458784 | tf_op jit(solution)/shard_map/all_to_all | solution.py:59
  348.1 3.5 all-to-all-start.1
  351.7 5.1 convolution_convert_fusion.2
  357.0 30.3 %all-gather.13.cloned.1.call-done = bf16[896,1536]{1,0:T(8,128)(2,1)} async-done(((bf16[112,1536]{1,0:T(8,128)(2,1)}), bf16[896,1536]{1,0:T(8,128)(2,1)}) %all-gather.13.cloned.1.call-update) | async-done | bytes 2752528 | tf_op jit(solution)/shard_map/all_gather | solution.py:62
  387.3 3.8 convolution_convert_fusion.1
  391.1 53.3 %all-gather.15.cloned.1.call-done = bf16[896,1536]{1,0:T(8,128)(2,1)} async-done(((bf16[112,1536]{1,0:T(8,128)(2,1)}), bf16[896,1536]{1,0:T(8,128)(2,1)}) %all-gather.15.cloned.1.call-update) | async-done | bytes 2752528 | tf_op jit(solution)/shard_map/all_gather | solution.py:63
  444.5 3.8 convolution_convert_fusion
  448.3 52.9 %all-gather.17.cloned.1.call-done = bf16[896,1536]{1,0:T(8,128)(2,1)} async-done(((bf16[112,1536]{1,0:T(8,128)(2,1)}), bf16[896,1536]{1,0:T(8,128)(2,1)}) %all-gather.17.cloned.1.call-update) | async-done | bytes 2752528 | tf_op jit(solution)/shard_map/all_gather | solution.py:64
  501.1 3.7 fusion
  505.1 16.9 %all-reduce.5.cloned.1.call-done = (bf16[112,2048]{1,0:T(8,128)(2,1)}, bf16[112,2048]{1,0:T(8,128)(2,1)}) async-done(((bf16[112,2048]{1,0:T(8,128)(2,1)}, bf16[112,2048]{1,0:T(8,128)(2,1)}), (bf16[112,2048]{1,0:T(8,128)(2,1)}, bf16[112,2048]{1,0:T(8,128)(2,1)})) %all-reduce.5.cloned.1.call-update) | async-done | bytes 917520 | tf_op jit(solution)/shard_map/psum | solution.py:38
  522.0 1.3 fusion.2
  523.3 2.5 fusion.5
  525.8 69.1 %all-reduce.7.cloned.1.call-done = (bf16[256,1536]{1,0:T(8,128)(2,1)}, bf16[256,1536]{1,0:T(8,128)(2,1)}, bf16[1536,256]{1,0:T(8,128)(2,1)}) async-done(((bf16[256,1536]{1,0:T(8,128)(2,1)}, bf16[256,1536]{1,0:T(8,128)(2,1)}, bf16[1536,256]{1,0:T(8,128)(2,1)}), (bf16[256,1536]{1,0:T(8,128)(2,1)}, bf16[256,1536]{1,0:T(8,128)(2,1)}, bf16[1536,256]{1,0:T(8,128)(2,1)})) %all-reduce.7.cloned.1.call-update) | async-done | bytes 2359312 | tf_op jit(solution)/shard_map/psum | solution.py:67
  594.9 3.1 convert_add_fusion
  598.0 3.3 convert_add_fusion.1
  (40 shorter events, 1.3 us)
Async XLA Ops:
  7.2 2.3 copy-start.1
  7.2 2.3 copy-start.2
  7.2 104.4 %all-gather.9.cloned.1.call-start = ((), (), s32[]{:S(2)}) async-start(), calls=%async_computation.3 | async-start | bytes 7077888 | tf_op jit(solution)/shard_map/all_gather | solution.py:24
  7.9 202.8 %all-gather.7.cloned.1.call-start = ((), (), s32[]{:S(2)}) async-start(), calls=%async_computation.2 | async-start | bytes 7077888 | tf_op jit(solution)/shard_map/all_gather | solution.py:23
  8.7 301.8 %all-gather.11.cloned.1.call-start = ((), (), s32[]{:S(2)}) async-start(), calls=%async_computation.4 | async-start | bytes 7077888 | tf_op jit(solution)/shard_map/all_gather | solution.py:25
  9.4 377.9 %all-gather.13.cloned.1.call-start = ((), (), s32[]{:S(2)}) async-start(), calls=%async_computation.5 | async-start | bytes 3096576 | tf_op jit(solution)/shard_map/all_gather | solution.py:62
  10.0 200.7 %copy-start.4 = (bf16[224,2048]{1,0:T(8,128)(2,1)}, bf16[224,2048]{1,0:T(8,128)(2,1)S(1)}, u32[]{:S(2)}) copy-start(bf16[224,2048]{1,0:T(8,128)(2,1)S(1)} %multiply_convert_fusion) | copy-start | bytes 2752516
  117.1 193.4 %copy-start = (bf16[112,2048]{1,0:T(8,128)(2,1)S(1)}, bf16[112,2048]{1,0:T(8,128)(2,1)}, u32[]{:S(2)}) copy-start(bf16[112,2048]{1,0:T(8,128)(2,1)} %param.11) | copy-start | bytes 1376260
  316.9 127.5 %all-gather.15.cloned.1.call-start = ((), (), s32[]{:S(2)}) async-start(), calls=%async_computation.6 | async-start | bytes 3096576 | tf_op jit(solution)/shard_map/all_gather | solution.py:63
  317.5 183.6 %all-gather.17.cloned.1.call-start = ((), (), s32[]{:S(2)}) async-start(), calls=%async_computation.7 | async-start | bytes 3096576 | tf_op jit(solution)/shard_map/all_gather | solution.py:64
  317.5 13.8 %slice-start = ((s8[6291456]{0:T(1024)(128)(4,1)}), s8[2097152]{0:T(1024)(128)(4,1)S(1)}, s32[]{:S(2)}) async-start(s8[6291456]{0:T(1024)(128)(4,1)} %bitcast.31), calls=%async_computation.10 | async-start | bytes 4194304
  321.3 26.8 %all-to-all-start = ((bf16[112,8,256]{2,0,1:T(8,128)(2,1)}), bf16[112,8,256]{2,0,1:T(8,128)(2,1)}, u32[]{:S(2)}, u32[]{:S(2)}) async-start(bf16[112,8,256]{2,0,1:T(8,128)(2,1)} %bitcast.35), calls=%async_computation | async-start | bytes 917504 | tf_op jit(solution)/shard_map/all_to_all | solution.py:59
  326.3 5.1 slice-start.1
  326.3 5.1 copy-start.3
  348.1 100.1 %all-to-all-start.1 = ((bf16[112,8,256]{2,0,1:T(8,128)(2,1)}), bf16[112,8,256]{2,0,1:T(8,128)(2,1)S(1)}, u32[]{:S(2)}, u32[]{:S(2)}) async-start(bf16[112,8,256]{2,0,1:T(8,128)(2,1)} %bitcast.34), calls=%async_computation.1 | async-start | bytes 917504 | tf_op jit(solution)/shard_map/all_to_all | solution.py:60
  351.6 170.3 %all-reduce.5.cloned.1.call-start = ((), (), s32[]{:S(2)}) async-start(), calls=%async_computation.8 | async-start | bytes 1835008 | tf_op jit(solution)/shard_map/psum | solution.py:38
  356.8 238.1 %all-reduce.7.cloned.1.call-start = ((), (), s32[]{:S(2)}) async-start(), calls=%async_computation.9 | async-start | bytes 4718592 | tf_op jit(solution)/shard_map/psum | solution.py:67
  594.9 3.1 copy-start.5
  594.9 3.1 copy-start.6
  594.9 3.1 copy-start.7
Sparse Core Ops, SparseCore 0:
  10.2 101.4 all-gather.8
  113.8 96.8 all-gather.6
  212.8 97.6 all-gather.10
  317.0 70.2 all-gather.12
  389.3 55.0 all-gather.14
  446.5 54.5 all-gather.16
  504.1 17.8 all-reduce.4
  525.0 69.9 all-reduce.6
where the time goes:
time: 609 us; the launch traced here: 608 us
  waiting for transfers between devices  528 us (87%)
  matrix products  42.7 us (7%)
  between operations  14.3 us (2%)
  other arithmetic  10.9 us (2%)
  starting transfers between devices  8.12 us (1%)
    all_gather x1, waiting for transfers between devices, shards(): lax.all_gather(w_up, 'fs', axis=0, tiled=True)  102 us
    all_gather x1, waiting for transfers between devices, shards(): lax.all_gather(w_gate, 'fs', axis=0, tiled=True)  93.6 us
    all_gather x1, waiting for transfers between devices, shards(): lax.all_gather(w_down, 'fs', axis=1, tiled=True)  93.2 us
    psum x1, waiting for transfers between devices, shards(): lax.psum(gate_delta.astype(jnp.bfloat16), 'rep').astype(jnp.float32)  69.1 us
    all_gather x1, waiting for transfers between devices, shards(): lax.all_gather(grad_up_in, 'fs', axis=0, tiled=True)  53.3 us
    all_gather x1, waiting for transfers between devices, shards(): lax.all_gather(early_hidden, 'fs', axis=0, tiled=True)  52.9 us
    all_gather x1, waiting for transfers between devices, shards(): lax.all_gather(grad_gate_in, 'fs', axis=0, tiled=True)  30.3 us
    psum x1, waiting for transfers between devices, shards(): branch = lax.psum(late_part, 'tp').astype(jnp.float32)  16.9 us
  transfers between devices with their start and end apart: 10, of which 9 were waited for; matrix products, arithmetic and copies ran while one was open for 7% of the time, Pallas kernels for 0%

commit v1 on v0

--- a/solution.py
+++ b/solution.py
@@ -64,7 +64,7 @@
     down_half = contract_rows(lax.all_gather(early_hidden, "fs", axis=0, tiled=True), out_cols)
     down_delta = 0.5 * down_half
     gate_delta, up_delta, down_delta = (
-        lax.psum(gate_delta.astype(jnp.bfloat16), "rep").astype(jnp.float32),
+        jnp.sum(lax.all_gather(gate_delta.astype(jnp.bfloat16), "rep"), axis=0).astype(jnp.float32),
         lax.psum(up_delta.astype(jnp.bfloat16), "rep").astype(jnp.float32),
         lax.psum(down_delta.astype(jnp.bfloat16), "rep").astype(jnp.float32),
     )

time: 609 us -> 612 us (level)
    all_gather x1, waiting for transfers between devices: 53.3 us -> 20.4 us  [shards(): lax.all_gather(grad_up_in, 'fs', axis=0, tiled=True)]
    all_gather x1, waiting for transfers between devices: 30.3 us -> 58.1 us  [shards(): lax.all_gather(grad_gate_in, 'fs', axis=0, tiled=True)]
    all_gather x0 -> x1, waiting for transfers between devices: none -> 24.9 us  [shards(): lax.all_gather(gate_delta.astype(jnp.bfloat16), 'rep')]
    psum x1, waiting for transfers between devices: 69.1 us -> 47.9 us  [shards(): lax.psum(up_delta.astype(jnp.bfloat16), 'rep').astype(jnp.float32)]
  transfers between devices with their start and end apart: 10 -> 11, of which waited for: 9 -> 10; matrix products, arithmetic and copies ran while one was open for 7% -> 8% of each run, Pallas kernels for 0% -> 0%
where the time goes in v1:
time: 612 us; the launch traced here: 611 us
  waiting for transfers between devices  534 us (87%)
  matrix products  42.2 us (7%)
  between operations  14 us (2%)
  other arithmetic  10.8 us (2%)
  starting transfers between devices  7.81 us (1%)
    all_gather x1, waiting for transfers between devices, shards(): lax.all_gather(w_up, 'fs', axis=0, tiled=True)  102 us
    all_gather x1, waiting for transfers between devices, shards(): lax.all_gather(w_gate, 'fs', axis=0, tiled=True)  93.6 us
    all_gather x1, waiting for transfers between devices, shards(): lax.all_gather(w_down, 'fs', axis=1, tiled=True)  93.4 us
    all_gather x1, waiting for transfers between devices, shards(): lax.all_gather(grad_gate_in, 'fs', axis=0, tiled=True)  58.1 us
    all_gather x1, waiting for transfers between devices, shards(): lax.all_gather(early_hidden, 'fs', axis=0, tiled=True)  54.5 us
    psum x1, waiting for transfers between devices, shards(): lax.psum(up_delta.astype(jnp.bfloat16), 'rep').astype(jnp.float32)  47.9 us
    all_gather x1, waiting for transfers between devices, shards(): lax.all_gather(gate_delta.astype(jnp.bfloat16), 'rep')  24.9 us
    all_gather x1, waiting for transfers between devices, shards(): lax.all_gather(grad_up_in, 'fs', axis=0, tiled=True)  20.4 us
  transfers between devices with their start and end apart: 11, of which 10 were waited for; matrix products, arithmetic and copies ran while one was open for 8% of the time, Pallas kernels for 0%

profile of v1, /device:TPU:0, one launch (start us, length us, event | category | flops | bytes accessed | tf_op | source)
XLA Modules:
  0.0 611.1 jit_solution(16582507389899302037)
XLA Ops:
  8.0 0.7 all-gather.9.cloned.1.call-update
  10.0 101.6 %all-gather.11.cloned.1.call-done = bf16[2048,1536]{1,0:T(8,128)(2,1)} async-done(((bf16[256,1536]{1,0:T(8,128)(2,1)}), bf16[2048,1536]{1,0:T(8,128)(2,1)}) %all-gather.11.cloned.1.call-update) | async-done | bytes 6291472 | tf_op jit(solution)/shard_map/all_gather | solution.py:24
  111.6 5.4 fusion.11
  117.1 93.6 %all-gather.9.cloned.1.call-done = bf16[2048,1536]{1,0:T(8,128)(2,1)} async-done(((bf16[256,1536]{1,0:T(8,128)(2,1)}), bf16[2048,1536]{1,0:T(8,128)(2,1)}) %all-gather.9.cloned.1.call-update) | async-done | bytes 6291472 | tf_op jit(solution)/shard_map/all_gather | solution.py:23
  210.7 6.3 %add_divide_fusion = (f32[224,1536]{1,0:T(8,128)}, bf16[224,1536]{1,0:T(8,128)(2,1)S(1)}, f32[224,1536]{1,0:T(8,128)}) fusion(f32[224,1536]{1,0:T(8,128)} %fusion.11, bf16[224,2048]{1,0:T(8,128)(2,1)S(1)} %multiply_convert_fusion, bf16[2048,1536]{1,0:T(8,128)(2,1)} %all-gather.9.cloned.1.call-done), kind=kOutput, calls=%fused_computation.14 | convolution fusion | flops 1411350528 | bytes 12025856 | tf_op jit(solution)/shard_map/dot_general | solution.py:31
  217.0 93.4 %all-gather.13.cloned.1.call-done = bf16[1536,2048]{1,0:T(8,128)(2,1)} async-done(((bf16[1536,256]{1,0:T(8,128)(2,1)}), bf16[1536,2048]{1,0:T(8,128)(2,1)}) %all-gather.13.cloned.1.call-update) | async-done | bytes 6291472 | tf_op jit(solution)/shard_map/all_gather | solution.py:25
  310.5 6.4 %multiply_convert_fusion.2 = (bf16[112,1536]{1,0:T(8,128)(2,1)}, bf16[112,1536]{1,0:T(8,128)(2,1)}) fusion(f32[224,1536]{1,0:T(8,128)} %get-tuple-element.15, f32[224,1536]{1,0:T(8,128)} %get-tuple-element.13, f32[224,1536]{1,0:T(8,128)} %fusion.11, bf16[112,2048]{1,0:T(8,128)(2,1)S(1)} %copy-done, bf16[1536,2048]{1,0:T(8,128)(2,1)} %all-gather.13.cloned.1.call-done), kind=kOutput, calls=%fused_computation.29 | convolution fusion | flops 706535424 | bytes 9502720 | tf_op jit(solution)/shard_map/dot_general | solution.py:16
  317.0 0.8 slice.44
  317.8 4.8 convolution_convert_fusion.2
  322.7 5.2 fusion.12
  327.9 2.8 fusion.1
  330.8 0.7 all-gather.15.cloned.1.call-update
  331.8 0.8 copy.24
  332.6 3.5 all-to-all-start
  336.0 0.8 copy.23
  336.8 19.6 %all-to-all-done = bf16[112,8,256]{2,0,1:T(8,128)(2,1)S(1)} async-done(((bf16[112,8,256]{2,0,1:T(8,128)(2,1)}), bf16[112,8,256]{2,0,1:T(8,128)(2,1)S(1)}, u32[]{:S(2)}, u32[]{:S(2)}) %all-to-all-start) | async-done | bytes 458784 | tf_op jit(solution)/shard_map/all_to_all | solution.py:59
  356.5 3.8 all-to-all-start.1
  360.3 20.4 %all-gather.17.cloned.1.call-done = bf16[896,1536]{1,0:T(8,128)(2,1)} async-done(((bf16[112,1536]{1,0:T(8,128)(2,1)}), bf16[896,1536]{1,0:T(8,128)(2,1)}) %all-gather.17.cloned.1.call-update) | async-done | bytes 2752528 | tf_op jit(solution)/shard_map/all_gather | solution.py:63
  380.7 3.7 convolution_convert_fusion
  384.4 54.5 %all-gather.19.cloned.1.call-done = bf16[896,1536]{1,0:T(8,128)(2,1)} async-done(((bf16[112,1536]{1,0:T(8,128)(2,1)}), bf16[896,1536]{1,0:T(8,128)(2,1)}) %all-gather.19.cloned.1.call-update) | async-done | bytes 2752528 | tf_op jit(solution)/shard_map/all_gather | solution.py:64
  438.9 3.7 fusion
  443.1 16.5 %all-reduce.5.cloned.1.call-done = (bf16[112,2048]{1,0:T(8,128)(2,1)}, bf16[112,2048]{1,0:T(8,128)(2,1)}) async-done(((bf16[112,2048]{1,0:T(8,128)(2,1)}, bf16[112,2048]{1,0:T(8,128)(2,1)}), (bf16[112,2048]{1,0:T(8,128)(2,1)}, bf16[112,2048]{1,0:T(8,128)(2,1)})) %all-reduce.5.cloned.1.call-update) | async-done | bytes 917520 | tf_op jit(solution)/shard_map/psum | solution.py:38
  459.6 1.3 fusion.2
  461.0 58.1 %all-gather.15.cloned.1.call-done = bf16[896,1536]{1,0:T(8,128)(2,1)} async-done(((bf16[112,1536]{1,0:T(8,128)(2,1)}), bf16[896,1536]{1,0:T(8,128)(2,1)}) %all-gather.15.cloned.1.call-update) | async-done | bytes 2752528 | tf_op jit(solution)/shard_map/all_gather | solution.py:62
  519.0 3.8 convolution_convert_fusion.1
  522.9 1.4 fusion.5
  524.2 47.9 %all-reduce.7.cloned.1.call-done = (bf16[256,1536]{1,0:T(8,128)(2,1)}, bf16[1536,256]{1,0:T(8,128)(2,1)}) async-done(((bf16[256,1536]{1,0:T(8,128)(2,1)}, bf16[1536,256]{1,0:T(8,128)(2,1)}), (bf16[256,1536]{1,0:T(8,128)(2,1)}, bf16[1536,256]{1,0:T(8,128)(2,1)})) %all-reduce.7.cloned.1.call-update) | async-done | bytes 1572880 | tf_op jit(solution)/shard_map/psum | solution.py:68
  572.1 3.1 convert_add_fusion
  575.2 1.4 convert_add_fusion.1
  576.6 24.9 %all-gather.21.cloned.1.call-done = bf16[512,1536]{1,0:T(8,128)(2,1)} async-done(((bf16[256,1536]{1,0:T(8,128)(2,1)}), bf16[512,1536]{1,0:T(8,128)(2,1)}) %all-gather.21.cloned.1.call-update) | async-done | bytes 1572880 | tf_op jit(solution)/shard_map/all_gather | solution.py:67
  601.5 1.7 reduce_sum.32
  603.2 1.3 convert_add_fusion.2
  (54 shorter events, 3.0 us)
Async XLA Ops:
  7.2 2.3 copy-start.1
  7.2 2.3 copy-start.2
  7.2 104.4 %all-gather.11.cloned.1.call-start = ((), (), s32[]{:S(2)}) async-start(), calls=%async_computation.3 | async-start | bytes 7077888 | tf_op jit(solution)/shard_map/all_gather | solution.py:24
  7.9 202.8 %all-gather.9.cloned.1.call-start = ((), (), s32[]{:S(2)}) async-start(), calls=%async_computation.2 | async-start | bytes 7077888 | tf_op jit(solution)/shard_map/all_gather | solution.py:23
  8.7 301.8 %all-gather.13.cloned.1.call-start = ((), (), s32[]{:S(2)}) async-start(), calls=%async_computation.4 | async-start | bytes 7077888 | tf_op jit(solution)/shard_map/all_gather | solution.py:25
  9.4 371.3 %all-gather.17.cloned.1.call-start = ((), (), s32[]{:S(2)}) async-start(), calls=%async_computation.6 | async-start | bytes 3096576 | tf_op jit(solution)/shard_map/all_gather | solution.py:63
  10.0 200.7 %copy-start.5 = (bf16[224,2048]{1,0:T(8,128)(2,1)}, bf16[224,2048]{1,0:T(8,128)(2,1)S(1)}, u32[]{:S(2)}) copy-start(bf16[224,2048]{1,0:T(8,128)(2,1)S(1)} %multiply_convert_fusion) | copy-start | bytes 2752516
  117.1 193.4 %copy-start = (bf16[112,2048]{1,0:T(8,128)(2,1)S(1)}, bf16[112,2048]{1,0:T(8,128)(2,1)}, u32[]{:S(2)}) copy-start(bf16[112,2048]{1,0:T(8,128)(2,1)} %param.11) | copy-start | bytes 1376260
  217.0 100.0 %copy-start.10 = (bf16[224,1536]{1,0:T(8,128)(2,1)}, bf16[224,1536]{1,0:T(8,128)(2,1)S(1)}, u32[]{:S(2)}) copy-start(bf16[224,1536]{1,0:T(8,128)(2,1)S(1)} %get-tuple-element.14) | copy-start | bytes 2064388
  316.9 122.0 %all-gather.19.cloned.1.call-start = ((), (), s32[]{:S(2)}) async-start(), calls=%async_computation.7 | async-start | bytes 3096576 | tf_op jit(solution)/shard_map/all_gather | solution.py:64
  317.8 141.8 %all-reduce.5.cloned.1.call-start = ((), (), s32[]{:S(2)}) async-start(), calls=%async_computation.9 | async-start | bytes 1835008 | tf_op jit(solution)/shard_map/psum | solution.py:38
  317.8 10.1 %slice-start = ((s8[6291456]{0:T(1024)(128)(4,1)}), s8[2097152]{0:T(1024)(128)(4,1)S(1)}, s32[]{:S(2)}) async-start(s8[6291456]{0:T(1024)(128)(4,1)} %bitcast.32), calls=%async_computation.11 | async-start | bytes 4194304
  322.6 5.2 slice-start.1
  322.7 5.2 copy-start.4
  330.7 1.0 slice-start.2
  330.8 188.3 %all-gather.15.cloned.1.call-start = ((), (), s32[]{:S(2)}) async-start(), calls=%async_computation.5 | async-start | bytes 3096576 | tf_op jit(solution)/shard_map/all_gather | solution.py:62
  332.6 23.9 %all-to-all-start = ((bf16[112,8,256]{2,0,1:T(8,128)(2,1)}), bf16[112,8,256]{2,0,1:T(8,128)(2,1)S(1)}, u32[]{:S(2)}, u32[]{:S(2)}) async-start(bf16[112,8,256]{2,0,1:T(8,128)(2,1)} %bitcast.31), calls=%async_computation | async-start | bytes 917504 | tf_op jit(solution)/shard_map/all_to_all | solution.py:59
  356.5 27.9 %copy-start.3 = (bf16[112,8,256]{2,0,1:T(8,128)(2,1)}, bf16[112,8,256]{2,0,1:T(8,128)(2,1)S(1)}, u32[]{:S(2)}) copy-start(bf16[112,8,256]{2,0,1:T(8,128)(2,1)S(1)} %all-to-all-done) | copy-start | bytes 1376260
  356.5 27.9 %all-to-all-start.1 = ((bf16[112,8,256]{2,0,1:T(8,128)(2,1)}), bf16[112,8,256]{2,0,1:T(8,128)(2,1)S(1)}, u32[]{:S(2)}, u32[]{:S(2)}) async-start(bf16[112,8,256]{2,0,1:T(8,128)(2,1)} %bitcast.30), calls=%async_computation.1 | async-start | bytes 917504 | tf_op jit(solution)/shard_map/all_to_all | solution.py:60
  360.3 211.9 %all-reduce.7.cloned.1.call-start = ((), (), s32[]{:S(2)}) async-start(), calls=%async_computation.10 | async-start | bytes 3145728 | tf_op jit(solution)/shard_map/psum | solution.py:68
  442.6 158.8 %all-gather.21.cloned.1.call-start = ((), (), s32[]{:S(2)}) async-start(), calls=%async_computation.8 | async-start | bytes 2359296 | tf_op jit(solution)/shard_map/all_gather | solution.py:67
  460.9 61.9 %copy-start.6 = (bf16[112,2048]{1,0:T(8,128)(2,1)S(1)}, bf16[112,2048]{1,0:T(8,128)(2,1)}, u32[]{:S(2)}) copy-start(bf16[112,2048]{1,0:T(8,128)(2,1)} %get-tuple-element.6) | copy-start | bytes 1376260
  460.9 61.9 %copy-start.11 = (bf16[112,2048]{1,0:T(8,128)(2,1)S(1)}, bf16[112,2048]{1,0:T(8,128)(2,1)}, u32[]{:S(2)}) copy-start(bf16[112,2048]{1,0:T(8,128)(2,1)} %get-tuple-element.5) | copy-start | bytes 1376260
  572.1 3.1 copy-start.7
  572.1 3.1 copy-start.9
  576.6 26.6 %copy-start.8 = (f32[256,1536]{1,0:T(8,128)S(1)}, f32[256,1536]{1,0:T(8,128)}, u32[]{:S(2)}) copy-start(f32[256,1536]{1,0:T(8,128)} %param.15) | copy-start | bytes 4718596
Sparse Core Ops, SparseCore 0:
  10.2 101.4 all-gather.10
  113.8 96.8 all-gather.8
  212.8 97.6 all-gather.12
  317.0 63.6 all-gather.16
  383.3 55.5 all-gather.18
  441.7 17.8 all-reduce.4
  461.8 57.1 all-gather.14
  522.0 50.1 all-reduce.6
  574.3 27.1 all-gather.20
